TPU v7x, 256 devices: a 4x2x16 block of a 4x16x16 slice. The times are simulated.
256 devices in a mesh: grp: 2 (over y), fs: 16 (over z), tp: 8 (over x, core).
Axes of the slice: x: 4, y: 2, z: 16, core: 2. Of those that a mesh axis runs over, the one named last changes fastest.
The devices are a block of a 4x16x16 slice.
Arguments:
- tokens: bfloat16 [32768, 2048], P(('grp', 'fs'), 'tp'), parts along dimension 0, may hold values from -50 to 50
- mix_gain: float32 [2048], replicated, may hold values from 0.1 to 1.9
- value_proj: bfloat16 [2048, 1024], P('fs', 'tp'), may hold values from -0.125 to 0.125
- gate_proj: bfloat16 [2048, 1024], P('fs', 'tp'), may hold values from -0.125 to 0.125
- conv_taps: float32 [31, 1024], P(None, 'tp'), may hold values from -1 to 1
- chan_gain: float32 [1024], replicated, may hold values from 0.1 to 1.9
- chan_shift: float32 [1024], replicated, may hold values from -3 to 3
- mix_out: bfloat16 [1024, 2048], P('fs', 'tp'), may hold values from -0.1875 to 0.1875
- mlp_gain: float32 [2048], replicated, may hold values from 0.1 to 1.9
- mlp_gate: bfloat16 [2048, 5632], P('fs', 'tp'), may hold values from -0.125 to 0.125
- mlp_up: bfloat16 [2048, 5632], P('fs', 'tp'), may hold values from -0.125 to 0.125
- gate_taps: float32 [3, 5632], P(None, 'tp'), may hold values from -3.5 to 3.5
- up_taps: float32 [3, 5632], P(None, 'tp'), may hold values from -3.5 to 3.5
- mlp_down: bfloat16 [5632, 2048], P('tp', 'fs'), may hold values from -0.078125 to 0.078125
- final_gain: float32 [2048], P('tp'), may hold values from 0.1 to 1.9
Outputs:
- layer_out: bfloat16 [32768, 2048], P(('grp', 'fs'), 'tp'), parts along dimension 0
There are 2 independent parts, one for each index of `grp`. A program takes and returns all parts, laid end to end along the dimension named above; an argument that names none is the same for every part. Nothing has to cross between parts.
All inputs are finite; a program needn't handle non-finite values.
Results may differ from a plain program's by a relative error of at most 0.0095.
Values may be sent and summed in bfloat16 or wider, within the bound.
A program may use at most 128 MiB of HBM per device.

v0:
```python
import jax
import jax.numpy as jnp
from jax import lax
from jax.sharding import PartitionSpec as P


def side_by_side(arrays, axis, dim, along):
    ends, at = ([], 0)
    for a in arrays[:-1]:
        at += a.shape[along]
        ends.append(at)
    both = jnp.concatenate(arrays, axis=along)
    return tuple(jnp.split(lax.all_gather(both, axis, axis=dim, tiled=True), ends, axis=along))


def rms_scale(values, gain):
    return values * lax.rsqrt(jnp.mean(values * values, axis=-1, keepdims=True) + 1e-06) * gain


def along_sequence(values, taps):
    width = taps.shape[0]
    half = (width - 1) // 2
    length = values.shape[0]
    padded = jnp.pad(values, ((half, width - 1 - half), (0, 0)))
    total = jnp.zeros_like(values)
    for offset in range(width):
        total = total + taps[offset] * padded[offset : offset + length]
    return total


def local(
    tokens,
    mix_gain,
    value_proj,
    gate_proj,
    conv_taps,
    chan_gain,
    chan_shift,
    mix_out,
    mlp_gain,
    mlp_gate,
    mlp_up,
    gate_taps,
    up_taps,
    mlp_down,
    final_gain,
):
    width_tp = lax.axis_size("tp")
    whole = lax.all_gather(tokens, "tp", axis=1, tiled=True)
    normed = rms_scale(whole.astype(jnp.float32), mix_gain).astype(jnp.bfloat16)
    first = jnp.dot(
        normed,
        lax.all_gather(value_proj, "fs", axis=0, tiled=True),
        preferred_element_type=jnp.float32,
    )
    second = jnp.dot(
        normed,
        lax.all_gather(gate_proj, "fs", axis=0, tiled=True),
        preferred_element_type=jnp.float32,
    )
    glu = first * jax.nn.sigmoid(second)
    conv_out = along_sequence(glu, conv_taps).astype(jnp.bfloat16)
    conv_all = lax.all_gather(conv_out, "tp", axis=1, tiled=True).astype(jnp.float32)
    mean = jnp.mean(conv_all, axis=-1, keepdims=True)
    var = jnp.mean(conv_all * conv_all, axis=-1, keepdims=True) - mean * mean
    chan_norm = (conv_all - mean) * lax.rsqrt(var + 1e-05) * chan_gain + chan_shift
    hidden_mix = jax.nn.silu(chan_norm).astype(jnp.bfloat16)
    mixer_result = jnp.dot(
        hidden_mix,
        lax.all_gather(mix_out, "fs", axis=0, tiled=True),
        preferred_element_type=jnp.float32,
    )
    mixed = (tokens.astype(jnp.float32) + mixer_result).astype(jnp.bfloat16)
    whole_two = lax.all_gather(mixed, "tp", axis=1, tiled=True)
    normed_two = rms_scale(whole_two.astype(jnp.float32), mlp_gain).astype(jnp.bfloat16)
    full_gate, full_up = side_by_side((mlp_gate, mlp_up), "fs", 0, 1)
    gate_pre = jnp.dot(normed_two, full_gate, preferred_element_type=jnp.float32)
    up_pre = jnp.dot(normed_two, full_up, preferred_element_type=jnp.float32)
    gate_conv = along_sequence(gate_pre, gate_taps)
    up_conv = along_sequence(up_pre, up_taps)
    hidden_mlp = (jax.nn.silu(gate_conv) * up_conv).astype(jnp.bfloat16)
    partial_terms = jnp.dot(
        hidden_mlp,
        lax.all_gather(mlp_down, "fs", axis=1, tiled=True),
        preferred_element_type=jnp.float32,
    )
    mlp_out = lax.psum_scatter(
        partial_terms.astype(jnp.bfloat16), "tp", scatter_dimension=1, tiled=True
    ).astype(jnp.float32)
    summed = mixed.astype(jnp.float32) + mlp_out
    squares = lax.psum(jnp.sum(summed * summed, axis=-1, keepdims=True), "tp")
    all_features = summed.shape[1] * width_tp
    layer_out = summed * lax.rsqrt(squares / all_features + 1e-06) * final_gain
    return layer_out.astype(jnp.bfloat16)


def solution(mesh):
    return jax.shard_map(
        local,
        mesh=mesh,
        in_specs=(
            P(("grp", "fs"), "tp"),
            P(),
            P("fs", "tp"),
            P("fs", "tp"),
            P(None, "tp"),
            P(),
            P(),
            P("fs", "tp"),
            P(),
            P("fs", "tp"),
            P("fs", "tp"),
            P(None, "tp"),
            P(None, "tp"),
            P("tp", "fs"),
            P("tp"),
        ),
        out_specs=P(("grp", "fs"), "tp"),
        check_vma=False,
    )
```

profile of v0, /device:TPU:33, one launch (start us, length us, event | category | flops | bytes accessed | tf_op | source)
XLA Modules:
  0.0 436.4 jit_solution(2931170777919696324)
XLA Ops:
  6.6 0.7 all-gather.6.cloned.1.call-update
  7.3 0.1 all-gather.8.cloned.1.call-start
  7.4 1.0 slice_bitcast_fusion.29
  8.3 1.0 slice_bitcast_fusion.30
  9.4 46.4 %all_gather.26 = bf16[2048,128]{1,0:T(8,128)(2,1)S(1)} all-gather(bf16[128,128]{1,0:T(8,128)(2,1)} %param.18), channel_id=1, replica_groups=mesh['grp'=2,'fs'=16,'tp'=8] {'fs'}, dimensions={0}, use_global_device_ids=true | all-gather | bytes 557056 | tf_op jit(solution)/shard_map/all_gather | solution.py:58
  55.7 23.2 %all_gather.25 = bf16[2048,128]{1,0:T(8,128)(2,1)S(1)} all-gather(bf16[128,128]{1,0:T(8,128)(2,1)} %param.17), channel_id=1, replica_groups=mesh['grp'=2,'fs'=16,'tp'=8] {'fs'}, dimensions={0}, use_global_device_ids=true | all-gather | bytes 557056 | tf_op jit(solution)/shard_map/all_gather | solution.py:53
  79.0 3.2 fusion
  82.2 0.2 copy-done.1
  82.4 1.3 fusion.41
  83.8 0.0 copy-start.3
  83.8 0.0 copy-start.6
  83.8 1.3 convolution_multiply_fusion
  85.1 0.0 copy-start.13
  85.1 0.0 copy-start.14
  85.1 2.8 add_convert_fusion
  87.9 0.1 all-gather.8.cloned.1.call-update
  88.0 0.1 all-gather.10.cloned.1.call-start
  88.1 0.2 copy.19
  88.3 23.6 %all_gather.28 = bf16[1024,256]{1,0:T(8,128)(2,1)S(1)} all-gather(bf16[64,256]{1,0:T(8,128)(2,1)S(1)} %copy-done.6), channel_id=1, replica_groups=mesh['grp'=2,'fs'=16,'tp'=8] {'fs'}, dimensions={0}, use_global_device_ids=true | all-gather | bytes 557056 | tf_op jit(solution)/shard_map/all_gather | solution.py:70
  111.9 16.1 %all-gather.8.cloned.1.call-done = bf16[1024,1024]{1,0:T(8,128)(2,1)} async-done(((bf16[1024,128]{1,0:T(8,128)(2,1)}), bf16[1024,1024]{1,0:T(8,128)(2,1)}) %all-gather.8.cloned.1.call-update) | async-done | bytes 2097168 | tf_op jit(solution)/shard_map/all_gather | solution.py:63
  128.1 2.3 convert_reduce_fusion
  130.4 0.0 copy-start.4
  130.4 0.0 copy-start.5
  130.4 0.0 copy-start.7
  130.4 0.0 copy-start.8
  130.4 4.4 %fusion.36 = bf16[1024,256]{0,1:T(8,128)(2,1)} fusion(bf16[1024,256]{1,0:T(8,128)(2,1)S(1)} %all_gather.28, bf16[1024,1024]{1,0:T(8,128)(2,1)} %all-gather.8.cloned.1.call-done, f32[1024]{0:T(1024)S(1)} %copy-done.13, f32[1024]{0:T(1024)S(1)} %copy-done.14, f32[1024]{0:T(1024)S(1)} %get-tuple-element.45, f32[1024]{0:T(1024)S(1)} %get-tuple-element.44, ...), kind=kOutput, calls=%fused_computation.44 | convolution fusion | flops 548143104 | bytes 3686400 | tf_op jit(solution)/shard_map/dot_general | solution.py:68
  134.8 0.1 all-gather.10.cloned.1.call-update
  134.9 0.1 all-gather.12.cloned.1.call-start
  135.0 0.8 pad_maximum_fusion
  135.8 0.1 all-gather.12.cloned.1.call-update
  135.8 0.1 all-gather.14.cloned.1.call-start
  135.9 0.6 all-gather.14.cloned.1.call-update
  136.5 0.2 reduce-scatter.2.cloned.1.call-start
  136.7 0.0 copy-done.7
  136.8 0.1 slice_reduce_fusion.2
  136.8 36.9 %all-gather.10.cloned.1.call-done = bf16[1024,2048]{0,1:T(8,128)(2,1)} async-done(((bf16[1024,256]{0,1:T(8,128)(2,1)}), bf16[1024,2048]{0,1:T(8,128)(2,1)}) %all-gather.10.cloned.1.call-update) | async-done | bytes 4194320 | tf_op jit(solution)/shard_map/all_gather | solution.py:74
  173.7 3.1 fusion.3
  176.8 93.9 %all-gather.12.cloned.1.call-done = bf16[2048,1408]{0,1:T(8,128)(2,1)} async-done(((bf16[128,1408]{0,1:T(8,128)(2,1)}), bf16[2048,1408]{0,1:T(8,128)(2,1)}) %all-gather.12.cloned.1.call-update) | async-done | bytes 5767184 | tf_op jit(solution)/shard_map/all_gather | solution.py:13
  270.7 6.4 %fusion.28 = f32[1024,704]{0,1:T(8,128)S(1)} fusion(bf16[2048,1408]{0,1:T(8,128)(2,1)} %all-gather.12.cloned.1.call-done, bf16[1024,2048]{0,1:T(8,128)(2,1)} %all-gather.10.cloned.1.call-done, f32[2048]{0:T(1024)S(1)} %copy-done.12, f32[1024]{0:T(1024)S(1)} %add_rsqrt_fusion.1), kind=kOutput, calls=%fused_computation.40 | convolution fusion | flops 2961178624 | bytes 9973760 | tf_op jit(solution)/shard_map/dot_general | solution.py:77
  277.1 4.8 %fusion.26 = f32[1024,704]{0,1:T(8,128)} fusion(bf16[2048,1408]{0,1:T(8,128)(2,1)S(1)} %copy-done.10, bf16[1024,2048]{0,1:T(8,128)(2,1)S(1)} %copy-done.2, f32[2048]{0:T(1024)S(1)} %copy-done.12, f32[1024]{0:T(1024)S(1)} %add_rsqrt_fusion.1), kind=kOutput, calls=%fused_computation.38 | convolution fusion | flops 2961178624 | bytes 9973760 | tf_op jit(solution)/shard_map/dot_general | solution.py:78
  282.0 68.3 %all-gather.14.cloned.1.call-done = bf16[704,2048]{1,0:T(8,128)(2,1)} async-done(((bf16[704,128]{1,0:T(8,128)(2,1)}), bf16[704,2048]{1,0:T(8,128)(2,1)}) %all-gather.14.cloned.1.call-update) | async-done | bytes 2883600 | tf_op jit(solution)/shard_map/all_gather | solution.py:84
  350.3 12.2 %convolution_convert_fusion = bf16[1024,2048]{0,1:T(8,128)(2,1)} fusion(bf16[704,2048]{1,0:T(8,128)(2,1)} %all-gather.14.cloned.1.call-done, f32[1024,704]{0,1:T(8,128)} %fusion.26, f32[1024,704]{0,1:T(8,128)S(1)} %fusion.28, f32[704]{0:T(1024)S(1)} %get-tuple-element.11, f32[704]{0:T(1024)S(1)} %get-tuple-element.12, f32[704]{0:T(1024)S(1)} %get-tuple-element.10, ...), kind=kOutput, calls=%fused_computation.23 | convolution fusion | flops 2966421504 | bytes 12861952 | tf_op jit(solution)/shard_map/dot_general | solution.py:82
  362.4 0.1 reduce-scatter.2.cloned.1.call-update
  362.5 48.7 %reduce-scatter.2.cloned.1.call-done = bf16[1024,256]{0,1:T(8,128)(2,1)} async-done(((bf16[1024,2048]{0,1:T(8,128)(2,1)}), bf16[1024,256]{0,1:T(8,128)(2,1)}) %reduce-scatter.2.cloned.1.call-update) | async-done | bytes 524304 | tf_op jit(solution)/shard_map/reduce_scatter | solution.py:87
  411.2 1.2 multiply_reduce_fusion
  412.4 14.8 %psum.7 = f32[1024,1]{0,1:T(1,128)S(1)} all-reduce(f32[1024,1]{0,1:T(1,128)S(1)} %bitcast.69), channel_id=1, replica_groups=mesh['grp'=2,'fs'=16,'tp'=8] {'tp'}, use_global_device_ids=true, to_apply=%region_6.7 | all-reduce | flops 1024 | bytes 8192 | tf_op jit(solution)/shard_map/psum | solution.py:91
  427.3 1.2 multiply_convert_fusion
  428.5 1.0 copy.21
  (26 shorter events, 0.1 us)
Async XLA Ops:
  6.5 75.7 %copy-start.11 = (f32[2048]{0:T(1024)S(1)}, f32[2048]{0:T(1024)}, u32[]{:S(2)}) copy-start(f32[2048]{0:T(1024)} %param.16) | copy-start | bytes 24580
  6.5 72.4 %all-gather.6.cloned.1.call-start = ((), (), s32[]{:S(2)}) async-start(), calls=%async_computation.1 | async-start | bytes 4718592 | tf_op jit(solution)/shard_map/all_gather | solution.py:49
  7.3 120.8 %all-gather.8.cloned.1.call-start = ((), (), s32[]{:S(2)}) async-start(), calls=%async_computation.2 | async-start | bytes 2359296 | tf_op jit(solution)/shard_map/all_gather | solution.py:63
  79.0 3.5 copy-start.1
  83.8 4.3 copy-start.3
  83.8 4.5 %copy-start.6 = (bf16[64,256]{1,0:T(8,128)(2,1)S(1)}, bf16[64,256]{1,0:T(8,128)(2,1)}, u32[]{:S(2)}) copy-start(bf16[64,256]{1,0:T(8,128)(2,1)} %param.22) | copy-start | bytes 98308
  85.1 45.2 %copy-start.13 = (f32[1024]{0:T(1024)S(1)}, f32[1024]{0:T(1024)}, u32[]{:S(2)}) copy-start(f32[1024]{0:T(1024)} %param.21) | copy-start | bytes 12292
  85.1 45.2 %copy-start.14 = (f32[1024]{0:T(1024)S(1)}, f32[1024]{0:T(1024)}, u32[]{:S(2)}) copy-start(f32[1024]{0:T(1024)} %param.20) | copy-start | bytes 12292
  88.0 85.7 %all-gather.10.cloned.1.call-start = ((), (), s32[]{:S(2)}) async-start(), calls=%async_computation.3 | async-start | bytes 4718592 | tf_op jit(solution)/shard_map/all_gather | solution.py:74
  130.4 4.6 %copy-start.4 = (bf16[128,704]{0,1:T(8,128)(2,1)S(1)}, bf16[128,704]{0,1:T(8,128)(2,1)}, u32[]{:S(2)}) copy-start(bf16[128,704]{0,1:T(8,128)(2,1)} %param.25) | copy-start | bytes 540676
  130.4 4.6 %copy-start.5 = (bf16[128,704]{0,1:T(8,128)(2,1)S(1)}, bf16[128,704]{0,1:T(8,128)(2,1)}, u32[]{:S(2)}) copy-start(bf16[128,704]{0,1:T(8,128)(2,1)} %param.24) | copy-start | bytes 540676
  130.4 6.3 %copy-start.7 = (f32[3,704]{1,0:T(4,128)S(1)}, f32[3,704]{1,0:T(4,128)}, u32[]{:S(2)}) copy-start(f32[3,704]{1,0:T(4,128)} %param.27) | copy-start | bytes 25348
  130.4 6.3 %copy-start.8 = (f32[3,704]{1,0:T(4,128)S(1)}, f32[3,704]{1,0:T(4,128)}, u32[]{:S(2)}) copy-start(f32[3,704]{1,0:T(4,128)} %param.26) | copy-start | bytes 25348
  134.8 135.8 %copy-start.12 = (f32[2048]{0:T(1024)S(1)}, f32[2048]{0:T(1024)}, u32[]{:S(2)}) copy-start(f32[2048]{0:T(1024)} %param.23) | copy-start | bytes 24580
  134.9 135.8 %all-gather.12.cloned.1.call-start = ((), (), s32[]{:S(2)}) async-start(), calls=%async_computation.4 | async-start | bytes 6127616 | tf_op jit(solution)/shard_map/all_gather | solution.py:13
  135.8 214.4 %all-gather.14.cloned.1.call-start = ((), (), s32[]{:S(2)}) async-start(), calls=%async_computation.5 | async-start | bytes 3063808 | tf_op jit(solution)/shard_map/all_gather | solution.py:84
  136.5 274.7 %reduce-scatter.2.cloned.1.call-start = ((), (), s32[]{:S(2)}) async-start(), calls=%async_computation.6 | async-start | bytes 4718592 | tf_op jit(solution)/shard_map/reduce_scatter | solution.py:87
  270.7 6.4 %copy-start.2 = (bf16[1024,2048]{0,1:T(8,128)(2,1)S(1)}, bf16[1024,2048]{0,1:T(8,128)(2,1)}, u32[]{:S(2)}) copy-start(bf16[1024,2048]{0,1:T(8,128)(2,1)} %all-gather.10.cloned.1.call-done) | copy-start | bytes 12582916
  270.7 6.5 %copy-start.10 = (bf16[2048,1408]{0,1:T(8,128)(2,1)S(1)}, bf16[2048,1408]{0,1:T(8,128)(2,1)}, u32[]{:S(2)}) copy-start(bf16[2048,1408]{0,1:T(8,128)(2,1)} %all-gather.12.cloned.1.call-done) | copy-start | bytes 17301508
  362.4 48.8 %copy-start = (bf16[1024,256]{0,1:T(8,128)(2,1)S(1)}, bf16[1024,256]{0,1:T(8,128)(2,1)}, u32[]{:S(2)}) copy-start(bf16[1024,256]{0,1:T(8,128)(2,1)} %fusion.36) | copy-start | bytes 1572868
  362.4 64.8 %copy-start.9 = (f32[256]{0:T(256)S(1)}, f32[256]{0:T(256)}, u32[]{:S(2)}) copy-start(f32[256]{0:T(256)} %param.29) | copy-start | bytes 3076
Sparse Core Ops, SparseCore 0:
  9.2 56.5 all-gather.5
  88.1 39.9 all-gather.7
  135.0 38.6 all-gather.9
  175.3 95.3 all-gather.11
  272.3 77.9 all-gather.13
  362.6 48.5 reduce-scatter.1
where the time goes:
time: 437 us; the launch traced here: 436 us
  waiting for transfers between devices  265 us (61%)
  blocking collectives  108 us (25%)
  matrix products  30.5 us (7%)
  other arithmetic  14.7 us (3%)
  between operations  13.7 us (3%)
    all_gather x1, waiting for transfers between devices, side_by_side(): lax.all_gather(both, axis, axis=dim, tiled=True)  93.9 us
    all_gather x1, waiting for transfers between devices, local(): lax.all_gather(mlp_down, 'fs', axis=1, tiled=True)  68.3 us
    reduce_scatter x1, waiting for transfers between devices, local(): lax.psum_scatter(partial_terms.astype(jnp.bfloat16), 'tp', scatter_dimens...  48.7 us
    all_gather x1, blocking collectives, local(): lax.all_gather(gate_proj, 'fs', axis=0, tiled=True)  46.4 us
    all_gather x1, waiting for transfers between devices, local(): whole_two = lax.all_gather(mixed, 'tp', axis=1, tiled=True)  36.9 us
    all_gather x1, blocking collectives, local(): lax.all_gather(mix_out, 'fs', axis=0, tiled=True)  23.6 us
    all_gather x1, blocking collectives, local(): lax.all_gather(value_proj, 'fs', axis=0, tiled=True)  23.2 us
    all_gather x1, waiting for transfers between devices, local(): lax.all_gather(conv_out, 'tp', axis=1, tiled=True).astype(jnp.float32)  16.1 us
  transfers between devices with their start and end apart: 6, of which 5 were waited for; matrix products, arithmetic and copies ran while one was open for 4% of the time, Pallas kernels for 0%

commit v1 on v0

--- a/solution.py
+++ b/solution.py
@@ -81,7 +81,9 @@
     hidden_mlp = (jax.nn.silu(gate_conv) * up_conv).astype(jnp.bfloat16)
     partial_terms = jnp.dot(
         hidden_mlp,
-        lax.all_gather(mlp_down, "fs", axis=1, tiled=True),
+        jnp.concatenate(
+            lax.all_to_all(jnp.stack([mlp_down] * lax.axis_size("fs")), "fs", 0, 0), axis=1
+        ),
         preferred_element_type=jnp.float32,
     )
     mlp_out = lax.psum_scatter(

time: 437 us -> 447 us (1.023)
  starting transfers between devices: 0.5 us -> 12.2 us
  waiting for transfers between devices: 265 us -> 259 us
    all_gather x1, waiting for transfers between devices: 93.9 us -> 174 us  [side_by_side(): lax.all_gather(both, axis, axis=dim, tiled=True)]
    all_gather x1 -> x0, waiting for transfers between devices: 68.3 us -> none  [local(): lax.all_gather(mlp_down, 'fs', axis=1, tiled=True)]
    all_gather x1, waiting for transfers between devices: 36.9 us -> 23.6 us  [local(): whole_two = lax.all_gather(mixed, 'tp', axis=1, tiled=True)]
    all_to_all x0 -> x1, starting transfers between devices: none -> 11.8 us  [local(): lax.all_to_all(jnp.stack([mlp_down] * lax.axis_size('fs')), 'fs', 0, 0)]
  transfers between devices with their start and end apart: 6 -> 6, of which waited for: 5 -> 4; matrix products, arithmetic and copies ran while one was open for 4% -> 5% of each run, Pallas kernels for 0% -> 0%
where the time goes in v1:
time: 447 us
  waiting for transfers between devices  259 us (58%)
  blocking collectives  108 us (24%)
  matrix products  33.4 us (7%)
  other arithmetic  14.7 us (3%)
  between operations  13.4 us (3%)
  starting transfers between devices  12.2 us (3%)
  local copies, waits for them, and re-layouts  5.64 us (1%)
    all_gather x1, waiting for transfers between devices, side_by_side(): lax.all_gather(both, axis, axis=dim, tiled=True)  174 us
    all_gather x1, blocking collectives, local(): lax.all_gather(gate_proj, 'fs', axis=0, tiled=True)  46.4 us
    reduce_scatter x1, waiting for transfers between devices, local(): lax.psum_scatter(partial_terms.astype(jnp.bfloat16), 'tp', scatter_dimens...  44.4 us
    all_gather x1, blocking collectives, local(): lax.all_gather(mix_out, 'fs', axis=0, tiled=True)  23.6 us
    all_gather x1, waiting for transfers between devices, local(): whole_two = lax.all_gather(mixed, 'tp', axis=1, tiled=True)  23.6 us
    all_gather x1, blocking collectives, local(): lax.all_gather(value_proj, 'fs', axis=0, tiled=True)  23.2 us
    all_gather x1, waiting for transfers between devices, local(): lax.all_gather(conv_out, 'tp', axis=1, tiled=True).astype(jnp.float32)  16.1 us
    psum x1, blocking collectives, local(): squares = lax.psum(jnp.sum(summed * summed, axis=-1, keepdims=True), 'tp')  14.8 us
  transfers between devices with their start and end apart: 6, of which 4 were waited for; matrix products, arithmetic and copies ran while one was open for 5% of the time, Pallas kernels for 0%

profile of v1, /device:TPU:33, one launch (start us, length us, event | category | flops | bytes accessed | tf_op | source)
XLA Modules:
  0.0 446.7 jit_solution(15566416436545558179)
XLA Ops:
  6.6 0.7 all-gather.5.cloned.1.call-update
  7.3 0.1 all-gather.7.cloned.1.call-start
  7.4 1.0 slice_bitcast_fusion.29
  8.3 1.0 slice_bitcast_fusion.30
  9.4 46.4 %all_gather.23 = bf16[2048,128]{1,0:T(8,128)(2,1)S(1)} all-gather(bf16[128,128]{1,0:T(8,128)(2,1)} %param.18), channel_id=1, replica_groups=mesh['grp'=2,'fs'=16,'tp'=8] {'fs'}, dimensions={0}, use_global_device_ids=true | all-gather | bytes 557056 | tf_op jit(solution)/shard_map/all_gather | solution.py:58
  55.7 23.2 %all_gather.22 = bf16[2048,128]{1,0:T(8,128)(2,1)S(1)} all-gather(bf16[128,128]{1,0:T(8,128)(2,1)} %param.17), channel_id=1, replica_groups=mesh['grp'=2,'fs'=16,'tp'=8] {'fs'}, dimensions={0}, use_global_device_ids=true | all-gather | bytes 557056 | tf_op jit(solution)/shard_map/all_gather | solution.py:53
  79.0 3.2 fusion
  82.2 0.2 copy-done.1
  82.4 1.3 fusion.43
  83.8 0.0 copy-start.3
  83.8 0.0 copy-start.7
  83.8 1.3 convolution_multiply_fusion
  85.1 0.0 copy-start.14
  85.1 0.0 copy-start.15
  85.1 2.8 add_convert_fusion
  87.9 0.1 all-gather.7.cloned.1.call-update
  88.0 0.1 all-gather.9.cloned.1.call-start
  88.1 0.2 copy.22
  88.3 23.6 %all_gather.25 = bf16[1024,256]{1,0:T(8,128)(2,1)S(1)} all-gather(bf16[64,256]{1,0:T(8,128)(2,1)S(1)} %copy-done.7), channel_id=1, replica_groups=mesh['grp'=2,'fs'=16,'tp'=8] {'fs'}, dimensions={0}, use_global_device_ids=true | all-gather | bytes 557056 | tf_op jit(solution)/shard_map/all_gather | solution.py:70
  111.9 16.1 %all-gather.7.cloned.1.call-done = bf16[1024,1024]{1,0:T(8,128)(2,1)} async-done(((bf16[1024,128]{1,0:T(8,128)(2,1)}), bf16[1024,1024]{1,0:T(8,128)(2,1)}) %all-gather.7.cloned.1.call-update) | async-done | bytes 2097168 | tf_op jit(solution)/shard_map/all_gather | solution.py:63
  128.1 2.3 convert_reduce_fusion
  130.4 0.0 copy-start.4
  130.4 0.0 copy-start.5
  130.4 0.0 copy-start.6
  130.4 4.4 fusion.38
  134.8 0.1 all-gather.9.cloned.1.call-update
  134.9 0.1 all-gather.11.cloned.1.call-start
  134.9 0.8 pad_maximum_fusion
  135.7 0.1 all-gather.11.cloned.1.call-update
  135.8 0.0 copy-start.8
  135.8 0.0 copy-start.9
  135.8 2.1 stack.2
  137.9 11.8 %all-to-all-start = ((bf16[16,704,128]{2,1,0:T(8,128)(2,1)}), bf16[16,704,128]{2,1,0:T(8,128)(2,1)S(1)}, u32[]{:S(2)}, u32[]{:S(2)}) async-start(bf16[16,704,128]{2,1,0:T(8,128)(2,1)} %stack.2), calls=%async_computation | async-start | bytes 5767168 | tf_op jit(solution)/shard_map/all_to_all | solution.py:85
  149.7 0.2 reduce-scatter.2.cloned.1.call-start
  150.0 0.1 slice_reduce_fusion.2
  150.1 23.6 %all-gather.9.cloned.1.call-done = bf16[1024,2048]{0,1:T(8,128)(2,1)} async-done(((bf16[1024,256]{0,1:T(8,128)(2,1)}), bf16[1024,2048]{0,1:T(8,128)(2,1)}) %all-gather.9.cloned.1.call-update) | async-done | bytes 4194320 | tf_op jit(solution)/shard_map/all_gather | solution.py:74
  173.7 3.1 fusion.3
  176.8 174.1 %all-gather.11.cloned.1.call-done = bf16[2048,1408]{0,1:T(8,128)(2,1)} async-done(((bf16[128,1408]{0,1:T(8,128)(2,1)}), bf16[2048,1408]{0,1:T(8,128)(2,1)}) %all-gather.11.cloned.1.call-update) | async-done | bytes 5767184 | tf_op jit(solution)/shard_map/all_gather | solution.py:13
  350.9 8.0 %fusion.30 = f32[1024,704]{0,1:T(8,128)} fusion(bf16[2048,1408]{0,1:T(8,128)(2,1)} %all-gather.11.cloned.1.call-done, bf16[1024,2048]{0,1:T(8,128)(2,1)} %all-gather.9.cloned.1.call-done, f32[2048]{0:T(1024)S(1)} %copy-done.13, f32[1024]{0:T(1024)S(1)} %add_rsqrt_fusion.1), kind=kOutput, calls=%fused_computation.42 | convolution fusion | flops 2961178624 | bytes 9973760 | tf_op jit(solution)/shard_map/dot_general | solution.py:77
  358.9 4.8 %fusion.28 = f32[1024,704]{0,1:T(8,128)} fusion(bf16[2048,1408]{0,1:T(8,128)(2,1)S(1)} %copy-done.11, bf16[1024,2048]{0,1:T(8,128)(2,1)S(1)} %copy-done.2, f32[2048]{0:T(1024)S(1)} %copy-done.13, f32[1024]{0:T(1024)S(1)} %add_rsqrt_fusion.1), kind=kOutput, calls=%fused_computation.40 | convolution fusion | flops 2961178624 | bytes 9973760 | tf_op jit(solution)/shard_map/dot_general | solution.py:78
  363.7 0.0 all-to-all-done
  363.7 13.6 %convolution_convert_fusion = bf16[1024,2048]{0,1:T(8,128)(2,1)} fusion(f32[1024,704]{0,1:T(8,128)} %fusion.28, f32[1024,704]{0,1:T(8,128)} %fusion.30, f32[704]{0:T(1024)S(1)} %get-tuple-element.11, f32[704]{0:T(1024)S(1)} %get-tuple-element.12, f32[704]{0:T(1024)S(1)} %get-tuple-element.10, f32[704]{0:T(1024)S(1)} %get-tuple-element.47, ...), kind=kOutput, calls=%fused_computation.23 | convolution fusion | flops 2966421504 | bytes 12861952 | tf_op jit(solution)/shard_map/dot_general | solution.py:82
  377.3 0.1 reduce-scatter.2.cloned.1.call-update
  377.4 44.4 %reduce-scatter.2.cloned.1.call-done = bf16[1024,256]{0,1:T(8,128)(2,1)} async-done(((bf16[1024,2048]{0,1:T(8,128)(2,1)}), bf16[1024,256]{0,1:T(8,128)(2,1)}) %reduce-scatter.2.cloned.1.call-update) | async-done | bytes 524304 | tf_op jit(solution)/shard_map/reduce_scatter | solution.py:89
  421.8 1.2 multiply_reduce_fusion
  423.0 14.8 %psum.7 = f32[1024,1]{0,1:T(1,128)S(1)} all-reduce(f32[1024,1]{0,1:T(1,128)S(1)} %bitcast.76), channel_id=1, replica_groups=mesh['grp'=2,'fs'=16,'tp'=8] {'tp'}, use_global_device_ids=true, to_apply=%region_6.7 | all-reduce | flops 1024 | bytes 8192 | tf_op jit(solution)/shard_map/psum | solution.py:93
  437.9 1.2 multiply_convert_fusion
  439.1 1.0 copy.25
  (28 shorter events, 0.1 us)
Async XLA Ops:
  6.5 75.7 %copy-start.12 = (f32[2048]{0:T(1024)S(1)}, f32[2048]{0:T(1024)}, u32[]{:S(2)}) copy-start(f32[2048]{0:T(1024)} %param.16) | copy-start | bytes 24580
  6.5 72.4 %all-gather.5.cloned.1.call-start = ((), (), s32[]{:S(2)}) async-start(), calls=%async_computation.2 | async-start | bytes 4718592 | tf_op jit(solution)/shard_map/all_gather | solution.py:49
  7.3 120.8 %all-gather.7.cloned.1.call-start = ((), (), s32[]{:S(2)}) async-start(), calls=%async_computation.3 | async-start | bytes 2359296 | tf_op jit(solution)/shard_map/all_gather | solution.py:63
  79.0 3.5 copy-start.1
  83.8 4.3 copy-start.3
  83.8 4.5 %copy-start.7 = (bf16[64,256]{1,0:T(8,128)(2,1)S(1)}, bf16[64,256]{1,0:T(8,128)(2,1)}, u32[]{:S(2)}) copy-start(bf16[64,256]{1,0:T(8,128)(2,1)} %param.22) | copy-start | bytes 98308
  85.1 45.2 %copy-start.14 = (f32[1024]{0:T(1024)S(1)}, f32[1024]{0:T(1024)}, u32[]{:S(2)}) copy-start(f32[1024]{0:T(1024)} %param.21) | copy-start | bytes 12292
  85.1 45.2 %copy-start.15 = (f32[1024]{0:T(1024)S(1)}, f32[1024]{0:T(1024)}, u32[]{:S(2)}) copy-start(f32[1024]{0:T(1024)} %param.20) | copy-start | bytes 12292
  88.0 85.7 %all-gather.9.cloned.1.call-start = ((), (), s32[]{:S(2)}) async-start(), calls=%async_computation.4 | async-start | bytes 4718592 | tf_op jit(solution)/shard_map/all_gather | solution.py:74
  130.4 4.6 %copy-start.4 = (bf16[128,704]{0,1:T(8,128)(2,1)S(1)}, bf16[128,704]{0,1:T(8,128)(2,1)}, u32[]{:S(2)}) copy-start(bf16[128,704]{0,1:T(8,128)(2,1)} %param.25) | copy-start | bytes 540676
  130.4 4.6 %copy-start.5 = (bf16[128,704]{0,1:T(8,128)(2,1)S(1)}, bf16[128,704]{0,1:T(8,128)(2,1)}, u32[]{:S(2)}) copy-start(bf16[128,704]{0,1:T(8,128)(2,1)} %param.24) | copy-start | bytes 540676
  130.4 5.4 %copy-start.6 = (bf16[704,128]{1,0:T(8,128)(2,1)S(1)}, bf16[704,128]{1,0:T(8,128)(2,1)}, u32[]{:S(2)}) copy-start(bf16[704,128]{1,0:T(8,128)(2,1)} %param.28) | copy-start | bytes 540676
  134.9 216.0 %all-gather.11.cloned.1.call-start = ((), (), s32[]{:S(2)}) async-start(), calls=%async_computation.5 | async-start | bytes 6127616 | tf_op jit(solution)/shard_map/all_gather | solution.py:13
  135.8 14.2 %copy-start.8 = (f32[3,704]{1,0:T(4,128)S(1)}, f32[3,704]{1,0:T(4,128)}, u32[]{:S(2)}) copy-start(f32[3,704]{1,0:T(4,128)} %param.27) | copy-start | bytes 25348
  135.8 14.2 %copy-start.9 = (f32[3,704]{1,0:T(4,128)S(1)}, f32[3,704]{1,0:T(4,128)}, u32[]{:S(2)}) copy-start(f32[3,704]{1,0:T(4,128)} %param.26) | copy-start | bytes 25348
  137.9 213.0 %copy-start.13 = (f32[2048]{0:T(1024)S(1)}, f32[2048]{0:T(1024)}, u32[]{:S(2)}) copy-start(f32[2048]{0:T(1024)} %param.23) | copy-start | bytes 24580
  137.9 225.8 %all-to-all-start = ((bf16[16,704,128]{2,1,0:T(8,128)(2,1)}), bf16[16,704,128]{2,1,0:T(8,128)(2,1)S(1)}, u32[]{:S(2)}, u32[]{:S(2)}) async-start(bf16[16,704,128]{2,1,0:T(8,128)(2,1)} %stack.2), calls=%async_computation | async-start | bytes 5767168 | tf_op jit(solution)/shard_map/all_to_all | solution.py:85
  149.7 272.1 %reduce-scatter.2.cloned.1.call-start = ((), (), s32[]{:S(2)}) async-start(), calls=%async_computation.6 | async-start | bytes 4718592 | tf_op jit(solution)/shard_map/reduce_scatter | solution.py:89
  350.9 8.0 %copy-start.2 = (bf16[1024,2048]{0,1:T(8,128)(2,1)S(1)}, bf16[1024,2048]{0,1:T(8,128)(2,1)}, u32[]{:S(2)}) copy-start(bf16[1024,2048]{0,1:T(8,128)(2,1)} %all-gather.9.cloned.1.call-done) | copy-start | bytes 12582916
  350.9 8.0 %copy-start.11 = (bf16[2048,1408]{0,1:T(8,128)(2,1)S(1)}, bf16[2048,1408]{0,1:T(8,128)(2,1)}, u32[]{:S(2)}) copy-start(bf16[2048,1408]{0,1:T(8,128)(2,1)} %all-gather.11.cloned.1.call-done) | copy-start | bytes 17301508
  377.3 44.5 %copy-start = (bf16[1024,256]{0,1:T(8,128)(2,1)S(1)}, bf16[1024,256]{0,1:T(8,128)(2,1)}, u32[]{:S(2)}) copy-start(bf16[1024,256]{0,1:T(8,128)(2,1)} %fusion.38) | copy-start | bytes 1572868
  377.3 60.6 %copy-start.10 = (f32[256]{0:T(256)S(1)}, f32[256]{0:T(256)}, u32[]{:S(2)}) copy-start(f32[256]{0:T(256)} %param.29) | copy-start | bytes 3076
Sparse Core Ops, SparseCore 0:
  9.2 56.5 all-gather.4
  88.1 39.9 all-gather.6
  135.0 38.6 all-gather.8
  175.3 175.5 all-gather.10
  377.5 44.2 reduce-scatter.1
